TPU v7x, 32 devices: a whole 2x2x4 slice. The times are simulated.
32 devices in a mesh: sp: 8 (over z, x), tp: 4 (over y, core).
Axes of the slice: x: 2, y: 2, z: 4, core: 2. Of those that a mesh axis runs over, the one named last changes fastest.
Arguments:
- tokens: bfloat16 [8192, 2048], P('sp'), may hold values from -8 to 8
- norm_gain: float32 [2048], replicated, may hold values from 0.1 to 1.9
- query_weight: bfloat16 [2048, 512], P(None, 'tp'), may hold values from -40 to 40
- key_weight: bfloat16 [2048, 256], P(None, 'tp'), may hold values from -1 to 1
- value_weight: bfloat16 [2048, 256], P(None, 'tp'), may hold values from -0.125 to 0.125
- sink_logits: float32 [8], P('tp'), may hold values from 1 to 6
- conv_in_weight: bfloat16 [2048, 512], P(None, 'tp'), may hold values from -0.125 to 0.125
- conv_gate_weight: bfloat16 [2048, 512], P(None, 'tp'), may hold values from -0.125 to 0.125
- conv_taps: bfloat16 [31, 512], replicated, may hold values from -1 to 1
- conv_gain: float32 [512], replicated, may hold values from 0.1 to 1.9
- point_weight: bfloat16 [512, 512], replicated, may hold values from -0.25 to 0.25
- output_gain: float32 [1024], replicated, may hold values from 0.1 to 1.9
- output_weight: bfloat16 [1024, 2048], P('sp'), may hold values from -0.1875 to 0.1875
Outputs:
- mixed_output: bfloat16 [8192, 2048], P(('sp', 'tp'))
All inputs are finite; a program needn't handle non-finite values.
Results may differ from a plain program's by a relative error of at most 0.0087.
Values may be sent and summed in bfloat16 or wider, within the bound.
A program may use at most 64 MiB of HBM per device.

v0:
```python
import jax
import jax.numpy as jnp
from jax import lax
from jax.sharding import PartitionSpec as P

HEADS = 8
KV_HEADS = 4
HEAD_DIM = 64
WINDOW = 128
CONV_WIDTH = 31


NORM_EPSILON = 1e-06
MASKED_SCORE = -1e30


def from_behind(block, axis, distance):
    devices = range(lax.axis_size(axis))
    route = [(i - distance, i) for i in devices if i - distance in devices]
    return lax.ppermute(block, axis, route)


def rms_rows(values, scale_gain):
    return (
        values
        * lax.rsqrt(jnp.mean(values * values, axis=-1, keepdims=True) + NORM_EPSILON)
        * scale_gain
    )


def depthwise(current, earlier_rows, tap_weights):
    extended = jnp.concatenate([earlier_rows, current], axis=0).astype(jnp.float32)
    tap_floats = tap_weights.astype(jnp.float32)
    row_count = current.shape[0]
    result = jnp.zeros(current.shape, jnp.float32)
    for tap_index in range(CONV_WIDTH):
        result = result + tap_floats[tap_index] * extended[tap_index : tap_index + row_count]
    return lax.optimization_barrier(result.astype(jnp.bfloat16))


def layer_activate(conv_rows, channel_gain):
    widened = conv_rows.astype(jnp.float32)
    centered = widened - jnp.mean(widened, axis=-1, keepdims=True)
    scaled = (
        centered
        * lax.rsqrt(jnp.mean(centered * centered, axis=-1, keepdims=True) + NORM_EPSILON)
        * channel_gain
    )
    return jax.nn.silu(scaled).astype(jnp.bfloat16)


def merge_groups(attended, pointwise, output_gain):
    head_width = attended.shape[1]
    return jnp.concatenate(
        [
            rms_rows(attended.astype(jnp.float32), output_gain[:head_width]),
            rms_rows(pointwise, output_gain[head_width:]),
        ],
        axis=1,
    ).astype(jnp.bfloat16)


def window_attention(queries, key_values, earlier_pairs, sinks_here, offset):
    row_count = queries.shape[0]
    block_count = row_count // WINDOW
    group_size = HEADS // KV_HEADS
    key_heads = key_values.shape[1] // (2 * HEAD_DIM)
    extended = jnp.concatenate([earlier_pairs, key_values], axis=0)
    extended = extended.reshape(block_count + 1, WINDOW, 2, key_heads, HEAD_DIM)
    key_value_band = jnp.concatenate([extended[:-1], extended[1:]], axis=1)
    key_band = key_value_band[:, :, 0]
    value_band = key_value_band[:, :, 1]
    grouped = queries.reshape(block_count, WINDOW, key_heads, group_size, HEAD_DIM)
    scores = jnp.einsum(
        "nqkgd,njkd->nkgqj", grouped, key_band, preferred_element_type=jnp.float32
    ) * HEAD_DIM ** (-0.5)
    query_index = lax.broadcasted_iota(jnp.int32, (WINDOW, 2 * WINDOW), 0)
    key_index = lax.broadcasted_iota(jnp.int32, (WINDOW, 2 * WINDOW), 1)
    distance = WINDOW + query_index - key_index
    in_window = (distance >= 0) & (distance < WINDOW)
    block_start = offset + jnp.arange(block_count, dtype=jnp.int32) * WINDOW - WINDOW
    allowed = in_window[None] & (block_start[:, None, None] + key_index[None] >= 0)
    scores = jnp.where(allowed[:, None, None], scores, MASKED_SCORE)
    sink_logit = sinks_here.reshape(key_heads, group_size)[None, :, :, None, None]
    row_peak = jnp.maximum(jnp.max(scores, axis=-1, keepdims=True), sink_logit)
    raised = jnp.exp(scores - row_peak)
    denominator = jnp.sum(raised, axis=-1, keepdims=True) + jnp.exp(sink_logit - row_peak)
    weights = (raised / denominator).astype(jnp.bfloat16)
    attended = jnp.einsum(
        "nkgqj,njkd->nqkgd", weights, value_band, preferred_element_type=jnp.float32
    )
    return attended.astype(jnp.bfloat16).reshape(row_count, key_heads * group_size * HEAD_DIM)


def on_device(
    tokens,
    norm_gain,
    query_weight,
    key_weight,
    value_weight,
    sink_logits,
    conv_in_weight,
    conv_gate_weight,
    conv_taps,
    conv_gain,
    point_weight,
    output_gain,
    output_weight,
):
    local_rows = tokens.shape[0]
    offset = lax.axis_index("sp") * local_rows
    normed = rms_rows(tokens.astype(jnp.float32), norm_gain).astype(jnp.bfloat16)
    queries = jnp.dot(normed, query_weight, preferred_element_type=jnp.float32).astype(jnp.bfloat16)
    key_part = jnp.dot(normed, key_weight, preferred_element_type=jnp.float32).astype(jnp.bfloat16)
    value_part = jnp.dot(normed, value_weight, preferred_element_type=jnp.float32).astype(
        jnp.bfloat16
    )
    key_values = jnp.concatenate([key_part, value_part], axis=1)
    conv_in = jnp.dot(normed, conv_in_weight, preferred_element_type=jnp.float32)
    conv_gate = jnp.dot(normed, conv_gate_weight, preferred_element_type=jnp.float32)
    gated_rows = (conv_in * jax.nn.sigmoid(conv_gate)).astype(jnp.bfloat16)
    earlier_pairs = from_behind(key_values[local_rows - WINDOW :], "sp", 1)
    attended = window_attention(queries, key_values, earlier_pairs, sink_logits, offset)
    head_rows, second_rows = (
        lax.all_to_all(attended, "tp", split_axis=0, concat_axis=1, tiled=True),
        lax.all_to_all(gated_rows, "tp", split_axis=0, concat_axis=1, tiled=True),
    )
    quarter_rows = second_rows.shape[0]
    earlier_quarter = from_behind(second_rows[quarter_rows - (CONV_WIDTH - 1) :], ("sp", "tp"), 1)
    conv_result = depthwise(second_rows, earlier_quarter, conv_taps)
    activated = layer_activate(conv_result, conv_gain)
    pointwise = jnp.dot(activated, point_weight, preferred_element_type=jnp.float32)
    merged = merge_groups(head_rows, pointwise, output_gain)
    projected = jnp.dot(
        merged,
        lax.all_gather(output_weight, "sp", axis=0, tiled=True),
        preferred_element_type=jnp.float32,
    )
    return projected.astype(jnp.bfloat16)


def solution(mesh):
    in_specs = (
        P("sp", None),
        P(),
        P(None, "tp"),
        P(None, "tp"),
        P(None, "tp"),
        P("tp"),
        P(None, "tp"),
        P(None, "tp"),
        P(),
        P(),
        P(),
        P(),
        P("sp", None),
    )
    out_specs = P(("sp", "tp"), None)
    return jax.shard_map(
        on_device, mesh=mesh, in_specs=in_specs, out_specs=out_specs, check_vma=False
    )
```

profile of v0, /device:TPU:0, one launch (start us, length us, event | category | flops | bytes accessed | tf_op | source)
XLA Modules:
  0.0 96.3 jit_solution(10529648924385393121)
XLA Ops:
  6.5 0.7 all-gather.2.cloned.1.call-update
  7.3 3.2 %fusion = f32[1024]{0:T(1024)S(1)} fusion(bf16[1024,2048]{1,0:T(8,128)(2,1)} %param.13), kind=kLoop, calls=%fused_computation.2 | loop fusion | flops 6290432 | bytes 4198400 | tf_op jit(solution)/shard_map/reduce_sum | solution.py:26
  10.7 1.0 %fusion.2 = bf16[1024,2048]{1,0:T(8,128)(2,1)S(1)} fusion(bf16[1024,2048]{1,0:T(8,128)(2,1)S(1)} %copy-done.2, f32[2048]{0:T(1024)S(1)} %copy-done.8, f32[1024]{0:T(1024)S(1)} %add_rsqrt_fusion), kind=kLoop, calls=%fused_computation.4 | loop fusion | flops 8388608 | bytes 8400896 | tf_op jit(solution)/shard_map/convert_element_type | solution.py:112
  11.8 1.4 %convolution_convert_fusion.3 = bf16[1024,64]{0,1:T(8,128)(2,1)S(1)} fusion(bf16[1024,2048]{1,0:T(8,128)(2,1)S(1)} %fusion.2, bf16[2048,64]{0,1:T(8,128)(2,1)S(1)} %copy-done.4), kind=kOutput, calls=%fused_computation.19 | convolution fusion | flops 268500992 | bytes 4587520 | tf_op jit(solution)/shard_map/dot_general | solution.py:115
  13.2 1.4 %convolution_convert_fusion.4 = bf16[1024,64]{0,1:T(8,128)(2,1)S(1)} fusion(bf16[1024,2048]{1,0:T(8,128)(2,1)S(1)} %fusion.2, bf16[2048,64]{0,1:T(8,128)(2,1)S(1)} %copy-done.5), kind=kOutput, calls=%fused_computation.20 | convolution fusion | flops 268500992 | bytes 4587520 | tf_op jit(solution)/shard_map/dot_general | solution.py:114
  14.6 5.0 %collective-permute-start = (bf16[128,128]{0,1:T(8,128)(2,1)S(1)}, bf16[128,128]{0,1:T(8,128)(2,1)S(1)}, u32[]{:S(2)}, u32[]{:S(2)}) collective-permute-start(bf16[128,128]{0,1:T(8,128)(2,1)S(1)} %fusion.67), channel_id=1, source_target_pairs={{0,4},{4,8},{8,12},{12,16},{16,20},{20,24},{24,28},{1,5},{5,9},{9,... | collective-permute-start | bytes 98312 | tf_op jit(solution)/shard_map/ppermute | solution.py:20
  19.6 1.3 %fusion.6 = f32[1024,128]{1,0:T(8,128)S(1)} fusion(bf16[1024,2048]{1,0:T(8,128)(2,1)S(1)} %fusion.2, bf16[2048,128]{1,0:T(8,128)(2,1)S(1)} %copy-done.11), kind=kOutput, calls=%fused_computation.14 | convolution fusion | flops 537264128 | bytes 5242880 | tf_op jit(solution)/shard_map/dot_general | solution.py:120
  20.9 1.3 %fusion.7 = bf16[1024,128]{1,0:T(8,128)(2,1)S(1)} fusion(f32[1024,128]{1,0:T(8,128)S(1)} %fusion.6, bf16[1024,2048]{1,0:T(8,128)(2,1)S(1)} %fusion.2, bf16[2048,128]{1,0:T(8,128)(2,1)S(1)} %copy-done.3), kind=kOutput, calls=%fused_computation.16 | convolution fusion | flops 537133056 | bytes 5505024 | tf_op jit(solution)/shard_map/dot_general | solution.py:119
  22.2 0.9 copy.36
  23.1 3.4 %all-to-all-start.1 = ((bf16[4,256,128]{1,2,0:T(8,128)(2,1)}), bf16[4,256,128]{1,2,0:T(8,128)(2,1)S(1)}, u32[]{:S(2)}, u32[]{:S(2)}) async-start(bf16[4,256,128]{1,2,0:T(8,128)(2,1)} %copy.36), calls=%async_computation.1 | async-start | bytes 524288 | tf_op jit(solution)/shard_map/all_to_all | solution.py:126
  26.7 1.0 %fusion.10 = pred[8,128,256]{1,2,0:T(8,128)(4,1)} fusion(s32[8]{0:T(128)S(1)} %add_add_fusion, pred[128,256]{0,1:T(8,128)(4,1)S(1)} %fusion.66), kind=kLoop, calls=%fused_computation.23 | loop fusion | flops 786432 | bytes 294944 | tf_op jit(solution)/shard_map/and | solution.py:82
  27.7 3.5 %convolution_convert_fusion.2 = bf16[1024,128]{1,0:T(8,128)(2,1)S(1)} fusion(bf16[1024,2048]{1,0:T(8,128)(2,1)} %copy-done.1, bf16[2048,128]{1,0:T(8,128)(2,1)S(1)} %copy-done.12), kind=kOutput, calls=%fused_computation.17 | convolution fusion | flops 537001984 | bytes 4980736 | tf_op jit(solution)/shard_map/dot_general | solution.py:113
  31.1 0.2 reshape.139
  31.8 1.7 %fusion.73 = (f32[8,2,128]{2,1,0:T(2,128)S(1)}, f32[8,1,2,128,256]{3,4,2,0,1:T(8,128)S(1)}) fusion(bf16[8,128,2,64]{3,2,1,0:T(2,128)(2,1)S(1)} %reshape.139, bf16[8,256,2,1,64]{1,4,0,3,2:T(8,128)(2,1)S(1)} %copy_dynamic-update-slice_fusion, pred[8,128,256]{1,2,0:T(8,128)(4,1)} %fusion.10), kind=kOutput, calls=%fused_computation.142 | convolution fusion | flops 68679680 | bytes 3153920 | tf_op jit(solution)/shard_map/nqkgd,njkd->nkgqj/dot_general | solution.py:74
  33.6 0.3 fusion.3
  34.2 2.3 %collective-permute-start.1 = (bf16[30,512]{1,0:T(8,128)(2,1)S(1)}, bf16[30,512]{1,0:T(8,128)(2,1)S(1)}, u32[]{:S(2)}, u32[]{:S(2)}) collective-permute-start(bf16[30,512]{1,0:T(8,128)(2,1)S(1)} %copy.45), channel_id=1, source_target_pairs={{0,1},{1,2},{2,3},{3,4},{4,5},{5,6},{6,7},{7,8},{8,9},{9,10},{10,1... | collective-permute-start | bytes 92168 | tf_op jit(solution)/shard_map/ppermute | solution.py:20
  36.5 1.4 %fusion.8 = bf16[8,128,1,2,64]{1,4,3,0,2:T(8,128)(2,1)S(1)} fusion(f32[8,1,2,128,256]{3,4,2,0,1:T(8,128)S(1)} %get-tuple-element.43, f32[8,2,128]{2,1,0:T(2,128)S(1)} %exponential_add_fusion, f32[8,2,128]{2,1,0:T(2,128)S(1)} %broadcast_maximum_fusion, bf16[8,256,2,1,64]{1,4,0,3,2:T(8,128)(2,1)} %copy-done.6), kind=kOutput, calls=%fused_computation.18 | convolution fusion | flops 68812800 | bytes 2637824 | tf_op jit(solution)/shard_map/nkgqj,njkd->nqkgd/dot_general | solution.py:89
  38.3 0.7 copy.34
  39.1 3.6 %all-to-all-start = ((bf16[4,256,128]{1,2,0:T(8,128)(2,1)}), bf16[4,256,128]{1,2,0:T(8,128)(2,1)S(1)}, u32[]{:S(2)}, u32[]{:S(2)}) async-start(bf16[4,256,128]{1,2,0:T(8,128)(2,1)} %copy.34), calls=%async_computation | async-start | bytes 524288 | tf_op jit(solution)/shard_map/all_to_all | solution.py:125
  43.0 6.9 %fusion.22 = bf16[256,512]{0,1:T(8,128)(2,1)S(1)} fusion(f32[286,512]{0,1:T(8,128)S(1)} %maximum_convert_fusion, f32[512]{0:T(512)S(1)} %bitcast.112, f32[512]{0:T(512)S(1)} %bitcast.111, f32[512]{0:T(512)S(1)} %bitcast.110, f32[512]{0:T(512)S(1)} %bitcast.109, f32[512]{0:T(512)S(1)} %bitcast.108, f32[512]{0:T(512)S(1)} %bitcast.107, f32[512]{0:T(512)S(1)} %bitcast.106, ...), kind=kLoop, calls=%fused_computation.38 | loop fusion | flops 8126464 | bytes 16578560 | tf_op jit(solution)/shard_map/convert_element_type | solution.py:38
  50.2 0.6 multiply_reduce_fusion
  51.0 0.2 copy.44
  51.4 33.6 %all-gather.2.cloned.1.call-done = bf16[1024,2048]{1,0:T(8,128)(2,1)} async-done(((bf16[128,2048]{1,0:T(8,128)(2,1)}), bf16[1024,2048]{1,0:T(8,128)(2,1)}) %all-gather.2.cloned.1.call-update) | async-done | bytes 4194320 | tf_op jit(solution)/shard_map/all_gather | solution.py:136
  85.0 4.4 %convolution_convert_fusion = bf16[256,2048]{1,0:T(8,128)(2,1)} fusion(bf16[1024,2048]{1,0:T(8,128)(2,1)} %all-gather.2.cloned.1.call-done, bf16[256,512]{1,0:T(8,128)(2,1)S(1)} %multiply_convert_fusion, bf16[256,512]{1,0:T(8,128)(2,1)S(1)} %multiply_convert_fusion.1), kind=kOutput, calls=%fused_computation.5 | convolution fusion | flops 1075314688 | bytes 5767168 | tf_op jit(solution)/shard_map/dot_general | solution.py:134
  (64 shorter events, 2.4 us)
Async XLA Ops:
  6.5 43.7 %copy-start = (bf16[512,512]{1,0:T(8,128)(2,1)S(1)}, bf16[512,512]{1,0:T(8,128)(2,1)}, u32[]{:S(2)}) copy-start(bf16[512,512]{1,0:T(8,128)(2,1)} %param.23) | copy-start | bytes 1572868
  6.5 4.0 %copy-start.8 = (f32[2048]{0:T(1024)S(1)}, f32[2048]{0:T(1024)}, u32[]{:S(2)}) copy-start(f32[2048]{0:T(1024)} %param.14) | copy-start | bytes 24580
  6.5 78.5 %all-gather.2.cloned.1.call-start = ((), (), s32[]{:S(2)}) async-start(), calls=%async_computation.2 | async-start | bytes 4718592 | tf_op jit(solution)/shard_map/all_gather | solution.py:136
  7.3 3.5 %copy-start.2 = (bf16[1024,2048]{1,0:T(8,128)(2,1)S(1)}, bf16[1024,2048]{1,0:T(8,128)(2,1)}, u32[]{:S(2)}) copy-start(bf16[1024,2048]{1,0:T(8,128)(2,1)} %param.13) | copy-start | bytes 12582916
  10.7 1.0 %copy-start.4 = (bf16[2048,64]{0,1:T(8,128)(2,1)S(1)}, bf16[2048,64]{0,1:T(8,128)(2,1)}, u32[]{:S(2)}) copy-start(bf16[2048,64]{0,1:T(8,128)(2,1)} %param.17) | copy-start | bytes 786436
  11.7 9.2 %copy-start.1 = (bf16[1024,2048]{1,0:T(8,128)(2,1)}, bf16[1024,2048]{1,0:T(8,128)(2,1)S(1)}, u32[]{:S(2)}) copy-start(bf16[1024,2048]{1,0:T(8,128)(2,1)S(1)} %fusion.2) | copy-start | bytes 12582916
  11.8 1.4 %copy-start.5 = (bf16[2048,64]{0,1:T(8,128)(2,1)S(1)}, bf16[2048,64]{0,1:T(8,128)(2,1)}, u32[]{:S(2)}) copy-start(bf16[2048,64]{0,1:T(8,128)(2,1)} %param.16) | copy-start | bytes 786436
  13.2 6.5 %copy-start.11 = (bf16[2048,128]{1,0:T(8,128)(2,1)S(1)}, bf16[2048,128]{1,0:T(8,128)(2,1)}, u32[]{:S(2)}) copy-start(bf16[2048,128]{1,0:T(8,128)(2,1)} %param.20) | copy-start | bytes 1572868
  14.6 6.3 %copy-start.3 = (bf16[2048,128]{1,0:T(8,128)(2,1)S(1)}, bf16[2048,128]{1,0:T(8,128)(2,1)}, u32[]{:S(2)}) copy-start(bf16[2048,128]{1,0:T(8,128)(2,1)} %param.19) | copy-start | bytes 1572868
  14.6 16.8 %collective-permute-start = (bf16[128,128]{0,1:T(8,128)(2,1)S(1)}, bf16[128,128]{0,1:T(8,128)(2,1)S(1)}, u32[]{:S(2)}, u32[]{:S(2)}) collective-permute-start(bf16[128,128]{0,1:T(8,128)(2,1)S(1)} %fusion.67), channel_id=1, source_target_pairs={{0,4},{4,8},{8,12},{12,16},{16,20},{20,24},{24,28},{1,5},{5,9},{9,... | collective-permute-start | bytes 98312 | tf_op jit(solution)/shard_map/ppermute | solution.py:20
  20.9 5.6 %copy-start.7 = (bf16[31,512]{1,0:T(8,128)(2,1)S(1)}, bf16[31,512]{1,0:T(8,128)(2,1)}, u32[]{:S(2)}) copy-start(bf16[31,512]{1,0:T(8,128)(2,1)} %param.21) | copy-start | bytes 95236
  20.9 6.7 %copy-start.12 = (bf16[2048,128]{1,0:T(8,128)(2,1)S(1)}, bf16[2048,128]{1,0:T(8,128)(2,1)}, u32[]{:S(2)}) copy-start(bf16[2048,128]{1,0:T(8,128)(2,1)} %param.15) | copy-start | bytes 1572868
  22.2 8.9 %copy-start.9 = (f32[1024]{0:T(1024)S(1)}, f32[1024]{0:T(1024)}, u32[]{:S(2)}) copy-start(f32[1024]{0:T(1024)} %param.24) | copy-start | bytes 12292
  23.1 10.9 %all-to-all-start.1 = ((bf16[4,256,128]{1,2,0:T(8,128)(2,1)}), bf16[4,256,128]{1,2,0:T(8,128)(2,1)S(1)}, u32[]{:S(2)}, u32[]{:S(2)}) async-start(bf16[4,256,128]{1,2,0:T(8,128)(2,1)} %copy.36), calls=%async_computation.1 | async-start | bytes 524288 | tf_op jit(solution)/shard_map/all_to_all | solution.py:126
  31.1 2.4 %copy-start.10 = (f32[2]{0:T(128)S(1)}, f32[2]{0:T(128)}, u32[]{:S(2)}) copy-start(f32[2]{0:T(128)} %param.18) | copy-start | bytes 28
  31.8 1.7 %copy-start.6 = (bf16[8,256,2,1,64]{1,4,0,3,2:T(8,128)(2,1)}, bf16[8,256,2,1,64]{1,4,0,3,2:T(8,128)(2,1)S(1)}, u32[]{:S(2)}) copy-start(bf16[8,256,2,1,64]{1,4,0,3,2:T(8,128)(2,1)S(1)} %copy_dynamic-update-slice_fusion) | copy-start | bytes 1572868
  34.2 8.5 %collective-permute-start.1 = (bf16[30,512]{1,0:T(8,128)(2,1)S(1)}, bf16[30,512]{1,0:T(8,128)(2,1)S(1)}, u32[]{:S(2)}, u32[]{:S(2)}) collective-permute-start(bf16[30,512]{1,0:T(8,128)(2,1)S(1)} %copy.45), channel_id=1, source_target_pairs={{0,1},{1,2},{2,3},{3,4},{4,5},{5,6},{6,7},{7,8},{8,9},{9,10},{10,1... | collective-permute-start | bytes 92168 | tf_op jit(solution)/shard_map/ppermute | solution.py:20
  39.1 11.9 %all-to-all-start = ((bf16[4,256,128]{1,2,0:T(8,128)(2,1)}), bf16[4,256,128]{1,2,0:T(8,128)(2,1)S(1)}, u32[]{:S(2)}, u32[]{:S(2)}) async-start(bf16[4,256,128]{1,2,0:T(8,128)(2,1)} %copy.34), calls=%async_computation | async-start | bytes 524288 | tf_op jit(solution)/shard_map/all_to_all | solution.py:125
  43.0 7.2 %copy-start.13 = (f32[512]{0:T(512)S(1)}, f32[512]{0:T(512)}, u32[]{:S(2)}) copy-start(f32[512]{0:T(512)} %param.22) | copy-start | bytes 6148
Sparse Core Ops, SparseCore 0:
  9.5 75.5 all-gather.1
where the time goes:
time: 96.7 us; the launch traced here: 96.3 us
  waiting for transfers between devices  34.3 us (35%)
  matrix products  16.9 us (17%)
  starting transfers between devices  14.3 us (15%)
  between operations  13.9 us (14%)
  other arithmetic  13.6 us (14%)
  local copies, waits for them, and re-layouts  3.29 us (3%)
    all_gather x1, waiting for transfers between devices, on_device(): lax.all_gather(output_weight, 'sp', axis=0, tiled=True)  33.6 us
    ppermute x2, starting transfers between devices, from_behind(): return lax.ppermute(block, axis, route)  7.34 us
    convert_element_type x1, other arithmetic, depthwise(): return lax.optimization_barrier(result.astype(jnp.bfloat16))  6.93 us
    dot_general x1, matrix products, on_device(): jnp.dot(merged, lax.all_gather(output_weight, 'sp', axis=0, tiled=True),...  4.41 us
    all_to_all x1, starting transfers between devices, on_device(): lax.all_to_all(attended, 'tp', split_axis=0, concat_axis=1, tiled=True)  3.59 us
    dot_general x1, matrix products, on_device(): jnp.dot(normed, query_weight, preferred_element_type=jnp.float32)  3.45 us
    all_to_all x1, starting transfers between devices, on_device(): lax.all_to_all(gated_rows, 'tp', split_axis=0, concat_axis=1, tiled=True)  3.4 us
    reduce_sum x2, other arithmetic, rms_rows(): jnp.mean(values * values, axis=-1, keepdims=True) + NORM_EPSILON  3.32 us
  transfers between devices with their start and end apart: 5, of which 1 were waited for; matrix products, arithmetic and copies ran while one was open for 30% of the time, Pallas kernels for 0%

commit v1 on v0

v1 whole, which is shorter than its diff:
```python
import functools

import jax
import jax.numpy as jnp
from jax import lax
from jax.experimental import pallas as pl
from jax.experimental.pallas import tpu as pltpu
from jax.sharding import PartitionSpec as P

HEAD_DIM = 64
WINDOW = 128
CONV_WIDTH = 31
HALO = 32
EPS = 1e-06
MASKED = -1e30
F32 = jnp.float32
BF16 = jnp.bfloat16
MESH = pl.DeviceIdType.MESH


def kernel(
    S, T,
    tok_hbm, ng, qw, kw, vw, sink, iw, gw, taps, cg, pw_hbm, og, ow_hbm,
    out,
    tok, wcat, kws, vws, pw, wfull, qb, kvb, g, a, ar, gr, ext, conv, act, mg,
    lsem, zsend, osend, xsend, ysend, csend, wrecv, hsend, hrecv, asend, arecv, gsend, grecv,
):
    s, t = lax.axis_index("sp"), lax.axis_index("tp")
    R, D = tok.shape
    Q = R // T
    Kl = ow_hbm.shape[0]
    Y, Z = T // 2, S // 2
    z, x = s // 2, lax.rem(s, 2)
    y, c = t // 2, lax.rem(t, 2)
    cw = D // T
    CC = g.shape[1]
    HW = a.shape[1]

    own = pl.ds(pl.multiple_of(s * Kl, Kl), Kl)
    loads = [pltpu.make_async_copy(ow_hbm, wfull.at[own], lsem.at[0])]
    loads += [
        pltpu.make_async_copy(qw, wcat.at[:, 0:HW], lsem.at[1]),
        pltpu.make_async_copy(kw, kws, lsem.at[2]),
        pltpu.make_async_copy(vw, vws, lsem.at[3]),
        pltpu.make_async_copy(iw, wcat.at[:, 2 * HW : 2 * HW + CC], lsem.at[4]),
        pltpu.make_async_copy(gw, wcat.at[:, 2 * HW + CC : 2 * HW + 2 * CC], lsem.at[5]),
        pltpu.make_async_copy(pw_hbm, pw, lsem.at[6]),
    ]
    tloads = [
        pltpu.make_async_copy(tok_hbm.at[q * Q : (q + 1) * Q], tok.at[q * Q : (q + 1) * Q], lsem.at[7 + q])
        for q in range(T)
    ]
    loads[0].start()
    tloads[T - 1].start()
    for i in range(1, 6):
        loads[i].start()
    for q in range(T - 2, -1, -1):
        tloads[q].start()
    loads[6].start()

    bar = pltpu.get_barrier_semaphore()

    def hello(ds_, dt_):
        pl.semaphore_signal(bar, inc=1, device_id=(ds_, dt_), device_id_type=MESH)

    for d in range(1, T):
        hello(s, lax.rem(t + d, T))
    hello(s + 1 - 2 * x, t)
    for step in (1, 2):
        @pl.when(s >= step)
        def _():
            hello(s - step, t)

        @pl.when(s + step < S)
        def _():
            hello(s + step, t)

    peers = T
    for step in (1, 2):
        peers = peers + jnp.where(s >= step, 1, 0) + jnp.where(s + step < S, 1, 0)
    pl.semaphore_wait(bar, peers)

    def piece(sh, col):
        return wfull.at[
            pl.ds(pl.multiple_of(sh * Kl, Kl), Kl), pl.ds(pl.multiple_of(col * cw, cw), cw)
        ]

    def send(sh, col, ds_, dt_, sem):
        ref = piece(sh, col)
        pltpu.make_async_remote_copy(
            src_ref=ref, dst_ref=ref, send_sem=sem, recv_sem=wrecv.at[sh, col],
            device_id=(ds_, dt_), device_id_type=MESH,
        ).start()

    def got(sh, col):
        ref = piece(sh, col)
        pltpu.make_async_copy(ref, ref, wrecv.at[sh, col]).wait()

    def sent(sem):
        ref = piece(0, 0)
        pltpu.make_async_copy(ref, ref, sem).wait()

    mycol = c * Y + y
    other_x = s + 1 - 2 * x
    sib = y * 2 + 1 - c

    def ycol(k):
        return c * Y + lax.rem(y + k, Y)

    def both(d):
        return ((z >= d, z - d, z + 1 < Z, 2), (z + d < Z, z + d, z >= 1, -2))

    def z_own():
        send(s, mycol, other_x, t, xsend.at[z])
        for k in range(Y):
            @pl.when(z + 1 < Z)
            def _():
                send(s, ycol(k), s + 2, t, zsend.at[z, k])

            @pl.when(z >= 1)
            def _():
                send(s, ycol(k), s - 2, t, osend.at[k])

    def z_step(d, k):
        for ok, zz, more, hop in both(d):
            @pl.when(ok)
            def _():
                sh = zz * 2 + x
                got(sh, ycol(k))

                @pl.when(more)
                def _():
                    send(sh, ycol(k), s + hop, t, zsend.at[zz, k])

                if k == 0:
                    send(sh, mycol, other_x, t, xsend.at[zz])
                send(sh, ycol(k), s, sib, csend.at[zz, k])

    def x_one(zz):
        sh = zz * 2 + 1 - x
        got(sh, mycol)
        for k in range(1, Y):
            send(sh, mycol, s, lax.rem(y + k, Y) * 2 + c, ysend.at[zz, k - 1])
        send(sh, mycol, s, sib, csend.at[zz, Y])

    def y_one(zz):
        sh = zz * 2 + 1 - x
        for k in range(1, Y):
            got(sh, ycol(k))
            send(sh, ycol(k), s, sib, csend.at[zz, Y + k])

    def at_distance(d, one):
        if d == 0:
            one(z)
        else:
            for ok, zz, _, _ in both(d):
                @pl.when(ok)
                def _():
                    one(zz)

    events = [
        functools.partial(z_step, 1, 0),
        functools.partial(at_distance, 0, x_one),
    ]
    for k in range(1, Y):
        events.append(functools.partial(z_step, 1, k))
    for d in range(2, Z + 2):
        if d < Z:
            events.append(functools.partial(z_step, d, 0))
        if d - 1 < Z:
            events.append(functools.partial(at_distance, d - 1, x_one))
        events.append(functools.partial(at_distance, d - 2, y_one))
        if d < Z:
            for k in range(1, Y):
                events.append(functools.partial(z_step, d, k))

    loads[0].wait()
    z_own()

    for i in range(1, 6):
        loads[i].wait()
    wcat[:, HW : 2 * HW] = jnp.concatenate([kws[...], vws[...]], axis=1)

    def send_gated(q):
        rows = pl.ds(q * Q, HALO + Q)

        @pl.when(t != q)
        def _():
            pltpu.make_async_remote_copy(
                src_ref=g.at[rows], dst_ref=gr.at[t], send_sem=gsend.at[q], recv_sem=grecv.at[t],
                device_id=(s, q), device_id_type=MESH,
            ).start()

    def halo(ref, n, i):
        return pltpu.make_async_remote_copy(
            src_ref=ref.at[pl.ds(R, n)], dst_ref=ref.at[pl.ds(0, n)],
            send_sem=hsend.at[i], recv_sem=hrecv.at[i],
            device_id=(lax.rem(s + 1, S), t), device_id_type=MESH,
        )

    def run(n):
        for _ in range(n):
            if events:
                events.pop(0)()

    for q in range(T - 1, -1, -1):
        tloads[q].wait()
        xs = tok[q * Q : (q + 1) * Q, :].astype(F32)
        scale = lax.rsqrt(jnp.mean(xs * xs, axis=-1, keepdims=True) + EPS)
        normed = (xs * scale * ng[...]).astype(BF16)
        p = jnp.dot(normed, wcat[...], preferred_element_type=F32)
        qb[q * Q : (q + 1) * Q, :] = (p[:, :HW] * HEAD_DIM ** (-0.5)).astype(BF16)
        kvb[WINDOW + q * Q : WINDOW + (q + 1) * Q, :] = p[:, HW : 2 * HW].astype(BF16)
        g[HALO + q * Q : HALO + (q + 1) * Q, :] = (
            p[:, 2 * HW : 2 * HW + CC] * jax.nn.sigmoid(p[:, 2 * HW + CC :])
        ).astype(BF16)
        if q == T - 1:
            @pl.when(s + 1 < S)
            def _():
                halo(kvb, WINDOW, 0).start()
                halo(g, HALO, 1).start()
        else:
            send_gated(q + 1)
        if q == T - 3:
            run(1)

    @pl.when(s == 0)
    def _():
        kvb[0:WINDOW, :] = jnp.zeros((WINDOW, kvb.shape[1]), BF16)
        g[0:HALO, :] = jnp.zeros((HALO, CC), BF16)

    @pl.when(s > 0)
    def _():
        halo(kvb, WINDOW, 0).wait_recv()
        halo(g, HALO, 1).wait_recv()

    send_gated(0)
    run(2)

    row = lax.broadcasted_iota(jnp.int32, (2 * WINDOW, 2 * WINDOW), 0)
    col = lax.broadcasted_iota(jnp.int32, (2 * WINDOW, 2 * WINDOW), 1)
    dist = WINDOW + lax.rem(row, WINDOW) - col
    inside = (dist >= 0) & (dist < WINDOW)
    head = lax.broadcasted_iota(jnp.int32, (2 * WINDOW, 1), 0) < WINDOW
    sinks = jnp.where(head, sink[0], sink[1])
    for i in range(T):
        q = lax.rem(t + 1 + i, T)
        for b in range(Q // WINDOW):
            base = pl.multiple_of(q * Q + b * WINDOW, WINDOW)
            rows = qb[pl.ds(base, WINDOW), :]
            kv = kvb[pl.ds(base, 2 * WINDOW), :]
            q2 = jnp.concatenate([rows[:, :HEAD_DIM], rows[:, HEAD_DIM:]], axis=0)
            sc = lax.dot_general(
                q2, kv[:, :HEAD_DIM], (((1,), (1,)), ((), ())), preferred_element_type=F32
            )
            low = jnp.where((s == 0) & (base == 0), WINDOW, 0)
            sc = jnp.where(inside & (col >= low), sc, MASKED)
            top = jnp.maximum(jnp.max(sc, axis=-1, keepdims=True), sinks)
            e = jnp.exp(sc - top)
            den = jnp.sum(e, axis=-1, keepdims=True) + jnp.exp(sinks - top)
            w = (e * (1.0 / den)).astype(BF16)
            o = jnp.dot(w, kv[:, HEAD_DIM:], preferred_element_type=F32).astype(BF16)
            a[pl.ds(base, WINDOW), :] = jnp.concatenate([o[:WINDOW], o[WINDOW:]], axis=1)
        if i < T - 1:
            pltpu.make_async_remote_copy(
                src_ref=a.at[pl.ds(pl.multiple_of(q * Q, Q), Q)], dst_ref=ar.at[t],
                send_sem=asend.at[i], recv_sem=arecv.at[t],
                device_id=(s, q), device_id_type=MESH,
            ).start()
        run(1)
    mine = pl.multiple_of(t * Q, Q)
    ar[t] = a[pl.ds(mine, Q), :]
    gr[t] = g[pl.ds(mine, HALO + Q), :]
    run(1)

    first = HALO - (CONV_WIDTH - 1)
    for d in range(1, T):
        p = lax.rem(t + d, T)
        pltpu.make_async_copy(gr.at[p], gr.at[p], grecv.at[p]).wait()
    total = jnp.zeros((Q, 1), F32)
    for p in range(T):
        ext[p] = gr[p].astype(F32)
        acc = jnp.zeros((Q, CC), F32)
        tp = taps[:, p * CC : (p + 1) * CC].astype(F32)
        for k in range(CONV_WIDTH):
            acc = acc + tp[k : k + 1] * ext[p, first + k : first + k + Q, :]
        rounded = acc.astype(BF16)
        conv[:, p * CC : (p + 1) * CC] = rounded
        if p == 1:
            run(1)
    run(1)
    cv = conv[...].astype(F32)
    cen = cv - jnp.mean(cv, axis=-1, keepdims=True)
    norm = cen * lax.rsqrt(jnp.mean(cen * cen, axis=-1, keepdims=True) + EPS) * cg[...]
    act[...] = (norm * jax.nn.sigmoid(norm)).astype(BF16)
    loads[6].wait()
    pt = jnp.dot(act[...], pw[...], preferred_element_type=F32)
    AW = T * HW
    mg[:, AW:] = (
        pt * lax.rsqrt(jnp.mean(pt * pt, axis=-1, keepdims=True) + EPS) * og[:, AW:]
    ).astype(BF16)
    run(1)
    for d in range(1, T):
        p = lax.rem(t + d, T)
        pltpu.make_async_copy(ar.at[p], ar.at[p], arecv.at[p]).wait()
    heads = jnp.concatenate([ar[p] for p in range(T)], axis=1).astype(F32)
    mg[:, :AW] = (
        heads * lax.rsqrt(jnp.mean(heads * heads, axis=-1, keepdims=True) + EPS) * og[:, :AW]
    ).astype(BF16)

    run(len(events))
    scol = [(1 - c) * Y + k for k in range(Y)]
    for d in range(Z):
        def rest(zz):
            for k in range(Y):
                if d > 0:
                    got(zz * 2 + x, scol[k])
                got(zz * 2 + 1 - x, scol[k])
        at_distance(d, rest)

    nb = 512
    for n in range(D // nb):
        out[:, n * nb : (n + 1) * nb] = jnp.dot(
            mg[...], wfull[:, n * nb : (n + 1) * nb], preferred_element_type=F32
        ).astype(BF16)

    sent(xsend.at[z])
    for k in range(Y):
        @pl.when(z + 1 < Z)
        def _():
            sent(zsend.at[z, k])

        @pl.when(z >= 1)
        def _():
            sent(osend.at[k])

    for d in range(Z):
        if d > 0:
            for ok, zz, more, _ in both(d):
                @pl.when(ok)
                def _():
                    for k in range(Y):
                        @pl.when(more)
                        def _():
                            sent(zsend.at[zz, k])
                        sent(csend.at[zz, k])
                    sent(xsend.at[zz])

        def done(zz):
            for k in range(1, Y):
                sent(ysend.at[zz, k - 1])
                sent(csend.at[zz, Y + k])
            sent(csend.at[zz, Y])
        at_distance(d, done)

    @pl.when(s + 1 < S)
    def _():
        halo(kvb, WINDOW, 0).wait_send()
        halo(g, HALO, 1).wait_send()

    for q in range(T):
        @pl.when(t != q)
        def _():
            pltpu.make_async_copy(gr.at[0], gr.at[0], gsend.at[q]).wait()
    for i in range(T - 1):
        pltpu.make_async_copy(ar.at[0], ar.at[0], asend.at[i]).wait()


def solution(mesh):
    S, T = mesh.shape["sp"], mesh.shape["tp"]

    def step(
        tokens, norm_gain, query_weight, key_weight, value_weight, sink_logits, conv_in_weight,
        conv_gate_weight, conv_taps, conv_gain, point_weight, output_gain, output_weight,
    ):
        R, D = tokens.shape
        Q = R // T
        HW, KW, CC = query_weight.shape[1], key_weight.shape[1], conv_in_weight.shape[1]
        C = point_weight.shape[0]
        MIX = output_gain.shape[0]
        Y, Z = T // 2, S // 2
        hbm = pl.BlockSpec(memory_space=pl.ANY)
        vmem = pl.BlockSpec(memory_space=pltpu.VMEM)
        smem = pl.BlockSpec(memory_space=pltpu.SMEM)
        dma = pltpu.SemaphoreType.DMA
        return pl.pallas_call(
            functools.partial(kernel, S, T),
            out_shape=jax.ShapeDtypeStruct((Q, D), BF16),
            in_specs=[hbm, vmem, hbm, hbm, hbm, smem, hbm, hbm, vmem, vmem, hbm, vmem, hbm],
            out_specs=vmem,
            scratch_shapes=[
                pltpu.VMEM((R, D), BF16),
                pltpu.VMEM((D, HW + 2 * KW + 2 * CC), BF16),
                pltpu.VMEM((D, KW), BF16),
                pltpu.VMEM((D, KW), BF16),
                pltpu.VMEM((C, C), BF16),
                pltpu.VMEM((MIX, D), BF16),
                pltpu.VMEM((R, HW), BF16),
                pltpu.VMEM((R + WINDOW, 2 * KW), BF16),
                pltpu.VMEM((R + HALO, CC), BF16),
                pltpu.VMEM((R, HW), BF16),
                pltpu.VMEM((T, Q, HW), BF16),
                pltpu.VMEM((T, Q + HALO, CC), BF16),
                pltpu.VMEM((T, Q + HALO, CC), F32),
                pltpu.VMEM((Q, C), BF16),
                pltpu.VMEM((Q, C), BF16),
                pltpu.VMEM((Q, MIX), BF16),
                dma((7 + T,)),
                dma((Z, Y)),
                dma((Y,)),
                dma((Z,)),
                dma((Z, Y - 1)),
                dma((Z, 2 * Y)),
                dma((S, T)),
                dma((2,)),
                dma((2,)),
                dma((T,)),
                dma((T,)),
                dma((T,)),
                dma((T,)),
            ],
            compiler_params=pltpu.CompilerParams(
                collective_id=0, has_side_effects=True, vmem_limit_bytes=56 * 1024 * 1024
            ),
        )(
            tokens, norm_gain[None], query_weight, key_weight, value_weight, sink_logits,
            conv_in_weight, conv_gate_weight, conv_taps, conv_gain[None], point_weight,
            output_gain[None], output_weight,
        )

    in_specs = (
        P("sp", None), P(), P(None, "tp"), P(None, "tp"), P(None, "tp"), P("tp"), P(None, "tp"),
        P(None, "tp"), P(), P(), P(), P(), P("sp", None),
    )
    return jax.shard_map(
        step, mesh=mesh, in_specs=in_specs, out_specs=P(("sp", "tp"), None), check_vma=False
    )
```

time: 96.7 us -> 40.8 us (0.42)
  the two profiles are of different devices: /device:TPU:0 before, /device:TPU:1 now
where the time goes in v1:
time: 40.8 us; the launch traced here: 40.5 us
  Pallas kernels  34.3 us (84%)
  local copies, waits for them, and re-layouts  6.23 us (15%)
    pallas_call x1, Pallas kernels, step(): pl.pallas_call(functools.partial(kernel, S, T), out_shape=jax.ShapeDtypeS...  34.3 us
    unnamed x3, local copies, waits for them, and re-layouts  6.23 us

profile of v1, /device:TPU:1, one launch (start us, length us, event | category | flops | bytes accessed | tf_op | source)
XLA Modules:
  0.0 40.5 jit_solution(3111205838507816291)
XLA Ops:
  0.0 2.0 %copy.14.kw = bf16[2048,64]{1,0:T(8,128)(2,1)} copy(bf16[2048,64]{0,1:T(8,128)(2,1)} %param.16) | data formatting | bytes 524288 | tf_op args[3]
  2.0 2.0 %copy.15.vw = bf16[2048,64]{1,0:T(8,128)(2,1)} copy(bf16[2048,64]{0,1:T(8,128)(2,1)} %param.17) | data formatting | bytes 524288 | tf_op args[4]
  3.9 34.3 %shard_map.127 = bf16[256,2048]{1,0:T(8,128)(2,1)} custom-call(bf16[1024,2048]{1,0:T(8,128)(2,1)} %tok_hbm.1, f32[1,2048]{1,0:T(1,128)} %bitcast.3, bf16[2048,128]{1,0:T(8,128)(2,1)} %qw.1, bf16[2048,64]{1,0:T(8,128)(2,1)} %copy.14.kw, bf16[2048,64]{1,0:T(8,128)(2,1)} %copy.15.vw, f32[2]{0:T(128)} %sink.1, bf16[2048,128]{1,0:T(8,128)(2,1)} %iw.1, ...), custom_call_target="tpu_custom_call" | custom-call | tf_op jit(solution)/shard_map/pallas_call | solution.py:386
  38.2 2.3 %copy.17 = bf16[256,2048]{1,0:T(8,128)(2,1)} copy(bf16[256,2048]{1,0:T(8,128)(2,1)} %shard_map.127) | data formatting | bytes 2097152

commit v2 on v1

--- a/solution.py
+++ b/solution.py
@@ -22,8 +22,8 @@
     S, T,
     tok_hbm, ng, qw, kw, vw, sink, iw, gw, taps, cg, pw_hbm, og, ow_hbm,
     out,
-    tok, wcat, kws, vws, pw, wfull, qb, kvb, g, a, ar, gr, ext, conv, act, mg,
-    lsem, zsend, osend, xsend, ysend, csend, wrecv, hsend, hrecv, asend, arecv, gsend, grecv,
+    tok, wcat, kvs, pw, wfull, qb, kvb, g, a, ar, gr, ext, conv, act, mg,
+    lsem, zsend, osend, psend, xsend, ysend, csend, wrecv, hsend, hrecv, asend, arecv, gsend, grecv,
 ):
     s, t = lax.axis_index("sp"), lax.axis_index("tp")
     R, D = tok.shape
@@ -32,7 +32,6 @@
     Y, Z = T // 2, S // 2
     z, x = s // 2, lax.rem(s, 2)
     y, c = t // 2, lax.rem(t, 2)
-    cw = D // T
     CC = g.shape[1]
     HW = a.shape[1]
 
@@ -40,8 +39,8 @@
     loads = [pltpu.make_async_copy(ow_hbm, wfull.at[own], lsem.at[0])]
     loads += [
         pltpu.make_async_copy(qw, wcat.at[:, 0:HW], lsem.at[1]),
-        pltpu.make_async_copy(kw, kws, lsem.at[2]),
-        pltpu.make_async_copy(vw, vws, lsem.at[3]),
+        pltpu.make_async_copy(kw, kvs.at[0 : kw.shape[0]], lsem.at[2]),
+        pltpu.make_async_copy(vw, kvs.at[kw.shape[0] : 2 * kw.shape[0]], lsem.at[3]),
         pltpu.make_async_copy(iw, wcat.at[:, 2 * HW : 2 * HW + CC], lsem.at[4]),
         pltpu.make_async_copy(gw, wcat.at[:, 2 * HW + CC : 2 * HW + 2 * CC], lsem.at[5]),
         pltpu.make_async_copy(pw_hbm, pw, lsem.at[6]),
@@ -80,74 +79,84 @@
         peers = peers + jnp.where(s >= step, 1, 0) + jnp.where(s + step < S, 1, 0)
     pl.semaphore_wait(bar, peers)
 
-    def piece(sh, col):
-        return wfull.at[
-            pl.ds(pl.multiple_of(sh * Kl, Kl), Kl), pl.ds(pl.multiple_of(col * cw, cw), cw)
-        ]
-
-    def send(sh, col, ds_, dt_, sem):
-        ref = piece(sh, col)
+    half, wide = D // 2, D // 4
+    narrow = wide // Y
+    other_x = s + 1 - 2 * x
+    sib = y * 2 + 1 - c
+
+    def piece(sh, cc, j):
+        rows = pl.ds(pl.multiple_of(sh * Kl, Kl), Kl)
+        if j is None:
+            return wfull.at[rows, pl.ds(pl.multiple_of(cc * half, wide), wide)]
+        return wfull.at[rows, pl.ds(pl.multiple_of(cc * half + wide + j * narrow, narrow), narrow)]
+
+    def slot(cc, j):
+        return cc * (Y + 1) + (0 if j is None else 1 + j)
+
+    def send(sh, j, ds_, dt_, sem):
+        ref = piece(sh, c, j)
         pltpu.make_async_remote_copy(
-            src_ref=ref, dst_ref=ref, send_sem=sem, recv_sem=wrecv.at[sh, col],
+            src_ref=ref, dst_ref=ref, send_sem=sem, recv_sem=wrecv.at[sh, slot(c, j)],
             device_id=(ds_, dt_), device_id_type=MESH,
         ).start()
 
-    def got(sh, col):
-        ref = piece(sh, col)
-        pltpu.make_async_copy(ref, ref, wrecv.at[sh, col]).wait()
-
-    def sent(sem):
-        ref = piece(0, 0)
+    def got(sh, cc, j):
+        ref = piece(sh, cc, j)
+        pltpu.make_async_copy(ref, ref, wrecv.at[sh, slot(cc, j)]).wait()
+
+    def sent(j, sem):
+        ref = piece(0, 0, j)
         pltpu.make_async_copy(ref, ref, sem).wait()
 
-    mycol = c * Y + y
-    other_x = s + 1 - 2 * x
-    sib = y * 2 + 1 - c
-
-    def ycol(k):
-        return c * Y + lax.rem(y + k, Y)
+    def yplane(k):
+        return lax.rem(y + k, Y)
 
     def both(d):
         return ((z >= d, z - d, z + 1 < Z, 2), (z + d < Z, z + d, z >= 1, -2))
 
+    def z_both(sh, j, i):
+        @pl.when(z + 1 < Z)
+        def _():
+            send(sh, j, s + 2, t, zsend.at[z, i])
+
+        @pl.when(z >= 1)
+        def _():
+            send(sh, j, s - 2, t, osend.at[i])
+
+    def across_y(sh, zz, i):
+        for k in range(1, Y):
+            send(sh, y, s, yplane(k) * 2 + c, ysend.at[zz, i * (Y - 1) + k - 1])
+
     def z_own():
-        send(s, mycol, other_x, t, xsend.at[z])
-        for k in range(Y):
-            @pl.when(z + 1 < Z)
-            def _():
-                send(s, ycol(k), s + 2, t, zsend.at[z, k])
-
-            @pl.when(z >= 1)
-            def _():
-                send(s, ycol(k), s - 2, t, osend.at[k])
-
-    def z_step(d, k):
+        send(s, y, other_x, t, psend.at[0])
+        z_both(s, None, 0)
+        send(s, None, other_x, t, xsend.at[z])
+        z_both(s, y, 1)
+
+    def crossed():
+        got(other_x, c, y)
+        z_both(other_x, y, 2)
+        across_y(other_x, z, 1)
+        send(other_x, y, s, sib, csend.at[z, Y + 2])
+
+    def z_step(d, i):
         for ok, zz, more, hop in both(d):
             @pl.when(ok)
             def _():
-                sh = zz * 2 + x
-                got(sh, ycol(k))
+                sh = zz * 2 + (1 - x if i == 2 else x)
+                j = None if i == 0 else y
+                got(sh, c, j)
 
                 @pl.when(more)
                 def _():
-                    send(sh, ycol(k), s + hop, t, zsend.at[zz, k])
-
-                if k == 0:
-                    send(sh, mycol, other_x, t, xsend.at[zz])
-                send(sh, ycol(k), s, sib, csend.at[zz, k])
-
-    def x_one(zz):
-        sh = zz * 2 + 1 - x
-        got(sh, mycol)
-        for k in range(1, Y):
-            send(sh, mycol, s, lax.rem(y + k, Y) * 2 + c, ysend.at[zz, k - 1])
-        send(sh, mycol, s, sib, csend.at[zz, Y])
-
-    def y_one(zz):
-        sh = zz * 2 + 1 - x
-        for k in range(1, Y):
-            got(sh, ycol(k))
-            send(sh, ycol(k), s, sib, csend.at[zz, Y + k])
+                    send(sh, j, s + hop, t, zsend.at[zz, i])
+
+                if i == 0:
+                    send(sh, j, other_x, t, xsend.at[zz])
+                    send(sh, j, s, sib, csend.at[zz, 0])
+                else:
+                    across_y(sh, zz, i - 1)
+                    send(sh, j, s, sib, csend.at[zz, (i - 1) * (Y + 1) + 1])
 
     def at_distance(d, one):
         if d == 0:
@@ -158,28 +167,34 @@
                 def _():
                     one(zz)
 
-    events = [
-        functools.partial(z_step, 1, 0),
-        functools.partial(at_distance, 0, x_one),
-    ]
-    for k in range(1, Y):
-        events.append(functools.partial(z_step, 1, k))
-    for d in range(2, Z + 2):
+    def x_one(zz):
+        sh = zz * 2 + 1 - x
+        got(sh, c, None)
+        send(sh, None, s, sib, csend.at[zz, Y + 1])
+
+    def y_one(d):
+        def one(zz):
+            for i in ((1,) if d == 0 else (0, 1)):
+                sh = zz * 2 + (x if i == 0 else 1 - x)
+                for k in range(1, Y):
+                    got(sh, c, yplane(k))
+                    send(sh, yplane(k), s, sib, csend.at[zz, i * (Y + 1) + 1 + k])
+        at_distance(d, one)
+
+    events = [crossed]
+    for d in range(1, Z + 1):
         if d < Z:
-            events.append(functools.partial(z_step, d, 0))
-        if d - 1 < Z:
-            events.append(functools.partial(at_distance, d - 1, x_one))
-        events.append(functools.partial(at_distance, d - 2, y_one))
-        if d < Z:
-            for k in range(1, Y):
-                events.append(functools.partial(z_step, d, k))
+            for i in range(3):
+                events.append(functools.partial(z_step, d, i))
+        events.append(functools.partial(at_distance, d - 1, x_one))
+        events.append(functools.partial(y_one, d - 1))
 
     loads[0].wait()
     z_own()
 
     for i in range(1, 6):
         loads[i].wait()
-    wcat[:, HW : 2 * HW] = jnp.concatenate([kws[...], vws[...]], axis=1)
+    wcat[:, HW : 2 * HW] = kvs[...].T
 
     def send_gated(q):
         rows = pl.ds(q * Q, HALO + Q)
@@ -221,8 +236,7 @@
                 halo(g, HALO, 1).start()
         else:
             send_gated(q + 1)
-        if q == T - 3:
-            run(1)
+        run(1 if q == T - 1 else 2 if q < T - 2 else 1)
 
     @pl.when(s == 0)
     def _():
@@ -235,7 +249,6 @@
         halo(g, HALO, 1).wait_recv()
 
     send_gated(0)
-    run(2)
 
     row = lax.broadcasted_iota(jnp.int32, (2 * WINDOW, 2 * WINDOW), 0)
     col = lax.broadcasted_iota(jnp.int32, (2 * WINDOW, 2 * WINDOW), 1)
@@ -267,7 +280,7 @@
                 send_sem=asend.at[i], recv_sem=arecv.at[t],
                 device_id=(s, q), device_id_type=MESH,
             ).start()
-        run(1)
+        run(2)
     mine = pl.multiple_of(t * Q, Q)
     ar[t] = a[pl.ds(mine, Q), :]
     gr[t] = g[pl.ds(mine, HALO + Q), :]
@@ -309,13 +322,12 @@
     ).astype(BF16)
 
     run(len(events))
-    scol = [(1 - c) * Y + k for k in range(Y)]
     for d in range(Z):
         def rest(zz):
-            for k in range(Y):
+            for j in (None, *range(Y)):
                 if d > 0:
-                    got(zz * 2 + x, scol[k])
-                got(zz * 2 + 1 - x, scol[k])
+                    got(zz * 2 + x, 1 - c, j)
+                got(zz * 2 + 1 - x, 1 - c, j)
         at_distance(d, rest)
 
     nb = 512
@@ -324,33 +336,33 @@
             mg[...], wfull[:, n * nb : (n + 1) * nb], preferred_element_type=F32
         ).astype(BF16)
 
-    sent(xsend.at[z])
-    for k in range(Y):
+    sent(0, psend.at[0])
+    for i in range(3):
+        j = None if i == 0 else 0
+
         @pl.when(z + 1 < Z)
         def _():
-            sent(zsend.at[z, k])
+            sent(j, zsend.at[z, i])
 
         @pl.when(z >= 1)
         def _():
-            sent(osend.at[k])
+            sent(j, osend.at[i])
+
+    for d in range(1, Z):
+        for ok, zz, more, _ in both(d):
+            @pl.when(ok & more)
+            def _():
+                for i in range(3):
+                    sent(None if i == 0 else 0, zsend.at[zz, i])
 
     for d in range(Z):
-        if d > 0:
-            for ok, zz, more, _ in both(d):
-                @pl.when(ok)
-                def _():
-                    for k in range(Y):
-                        @pl.when(more)
-                        def _():
-                            sent(zsend.at[zz, k])
-                        sent(csend.at[zz, k])
-                    sent(xsend.at[zz])
-
         def done(zz):
-            for k in range(1, Y):
-                sent(ysend.at[zz, k - 1])
-                sent(csend.at[zz, Y + k])
-            sent(csend.at[zz, Y])
+            sent(None, xsend.at[zz])
+            for i in ((1,) if d == 0 else (0, 1)):
+                for k in range(1, Y):
+                    sent(0, ysend.at[zz, i * (Y - 1) + k - 1])
+                for k in range(Y + 1):
+                    sent(None if k == 0 else 0, csend.at[zz, i * (Y + 1) + k])
         at_distance(d, done)
 
     @pl.when(s + 1 < S)
@@ -391,8 +403,7 @@
             scratch_shapes=[
                 pltpu.VMEM((R, D), BF16),
                 pltpu.VMEM((D, HW + 2 * KW + 2 * CC), BF16),
-                pltpu.VMEM((D, KW), BF16),
-                pltpu.VMEM((D, KW), BF16),
+                pltpu.VMEM((2 * KW, D), BF16),
                 pltpu.VMEM((C, C), BF16),
                 pltpu.VMEM((MIX, D), BF16),
                 pltpu.VMEM((R, HW), BF16),
@@ -406,12 +417,13 @@
                 pltpu.VMEM((Q, C), BF16),
                 pltpu.VMEM((Q, MIX), BF16),
                 dma((7 + T,)),
-                dma((Z, Y)),
-                dma((Y,)),
+                dma((Z, 3)),
+                dma((3,)),
+                dma((1,)),
                 dma((Z,)),
-                dma((Z, Y - 1)),
-                dma((Z, 2 * Y)),
-                dma((S, T)),
+                dma((Z, 2 * (Y - 1))),
+                dma((Z, 2 * (Y + 1))),
+                dma((S, 2 * (Y + 1))),
                 dma((2,)),
                 dma((2,)),
                 dma((T,)),
@@ -423,7 +435,7 @@
                 collective_id=0, has_side_effects=True, vmem_limit_bytes=56 * 1024 * 1024
             ),
         )(
-            tokens, norm_gain[None], query_weight, key_weight, value_weight, sink_logits,
+            tokens, norm_gain[None], query_weight, key_weight.T, value_weight.T, sink_logits,
             conv_in_weight, conv_gate_weight, conv_taps, conv_gain[None], point_weight,
             output_gain[None], output_weight,
         )

time: 40.8 us -> 33.7 us (0.83)
  local copies, waits for them, and re-layouts: 6.23 us -> 2.3 us
  Pallas kernels: 34.3 us -> 31.2 us
    unnamed x3 -> x1, local copies, waits for them, and re-layouts: 6.23 us -> 2.3 us
    pallas_call x1, Pallas kernels: 34.3 us -> 31.2 us  [step(): pl.pallas_call(functools.partial(kernel, S, T), out_shape=jax.ShapeDtypeS...]
where the time goes in v2:
time: 33.7 us; the launch traced here: 33.5 us
  Pallas kernels  31.2 us (93%)
  local copies, waits for them, and re-layouts  2.3 us (7%)
    pallas_call x1, Pallas kernels, step(): pl.pallas_call(functools.partial(kernel, S, T), out_shape=jax.ShapeDtypeS...  31.2 us
    unnamed x1, local copies, waits for them, and re-layouts  2.3 us

profile of v2, /device:TPU:1, one launch (start us, length us, event | category | flops | bytes accessed | tf_op | source)
XLA Modules:
  0.0 33.5 jit_solution(857915333528263989)
XLA Ops:
  0.0 31.2 %shard_map.127 = bf16[256,2048]{1,0:T(8,128)(2,1)} custom-call(bf16[1024,2048]{1,0:T(8,128)(2,1)} %tok_hbm.1, f32[1,2048]{1,0:T(1,128)} %bitcast.7, bf16[2048,128]{1,0:T(8,128)(2,1)} %qw.1, bf16[64,2048]{1,0:T(8,128)(2,1)} %bitcast.5, bf16[64,2048]{1,0:T(8,128)(2,1)} %bitcast.6, f32[2]{0:T(128)} %sink.1, bf16[2048,128]{1,0:T(8,128)(2,1)} %iw.1, ...), custom_call_target="tpu_custom_call" | custom-call | tf_op jit(solution)/shard_map/pallas_call | solution.py:398
  31.2 2.3 %copy.15 = bf16[256,2048]{1,0:T(8,128)(2,1)} copy(bf16[256,2048]{1,0:T(8,128)(2,1)} %shard_map.127) | data formatting | bytes 2097152
